TPU v7x, 32 devices: a whole 2x2x4 slice. The times are simulated.
32 devices in a mesh: grp: 2 (over y), fs: 4 (over z), tp: 4 (over x, core).
Axes of the slice: x: 2, y: 2, z: 4, core: 2. Of those that a mesh axis runs over, the one named last changes fastest.
Arguments:
- tokens: bfloat16 [2048, 3072], P(('grp', 'tp')), parts along dimension 0, may hold values from -6 to 6
- up_master: float32 [3072, 12288], P('fs', 'tp'), may hold values from -0.109375 to 0.109375
- down_master: float32 [12288, 3072], P('fs', 'tp'), may hold values from -0.0546875 to 0.0546875
- norm_gain: float32 [3072], P('fs'), may hold values from 0.1 to 1.9
Outputs:
- prompt_out: bfloat16 [2048, 3072], P(('grp', 'tp'), 'fs'), parts along dimension 0
- sampled_up: bfloat16 [6144, 12288], P('grp', 'fs'), parts along dimension 0
- sampled_down: bfloat16 [24576, 3072], P(('grp', 'fs')), parts along dimension 0
There are 2 independent parts, one for each index of `grp`. A program takes and returns all parts, laid end to end along the dimension named above; an argument that names none is the same for every part. Nothing has to cross between parts.
All inputs are finite; a program needn't handle non-finite values.
Results may differ from a plain program's by a relative error of at most 0.0074.
Values may be sent and summed in bfloat16 or wider, within the bound.
A program may use at most 192 MiB of HBM per device.

v0:
```python
import jax
import jax.numpy as jnp
from jax import lax
from jax.sharding import PartitionSpec as P


def normalize(tokens):
    values = tokens.astype(jnp.float32)
    center = jnp.mean(values, axis=-1, keepdims=True)
    spread = jnp.mean(jnp.square(values - center), axis=-1, keepdims=True)
    return ((values - center) * lax.rsqrt(spread + 1e-05)).astype(jnp.bfloat16)


def shards(tokens, up_master, down_master, norm_gain):
    up_cast = (norm_gain[:, None] * up_master).astype(jnp.bfloat16)
    down_cast = down_master.astype(jnp.bfloat16)
    quarter = lax.all_to_all(up_cast, "tp", split_axis=0, concat_axis=1, tiled=True)
    moved = lax.all_to_all(quarter, "fs", split_axis=1, concat_axis=0, tiled=True)
    part_rows = quarter.shape[0]
    stacked = moved.reshape(moved.shape[0] // part_rows, part_rows, moved.shape[1])
    joined, sampled_down = (
        lax.all_gather(stacked, "tp", axis=1, tiled=True),
        lax.all_gather(down_cast, "tp", axis=1, tiled=True),
    )
    sampled_up = joined.reshape(joined.shape[0] * joined.shape[1], joined.shape[2])
    normalized = normalize(tokens)
    before = jnp.dot(normalized, sampled_up, preferred_element_type=jnp.float32)
    hidden = jnp.square(jax.nn.relu(before)).astype(jnp.bfloat16)
    terms = jnp.dot(hidden, sampled_down, preferred_element_type=jnp.float32)
    summed = lax.psum_scatter(terms, "fs", scatter_dimension=1, tiled=True)
    return (summed.astype(jnp.bfloat16), sampled_up, sampled_down)


def solution(mesh):
    return jax.shard_map(
        shards,
        mesh=mesh,
        in_specs=(P(("grp", "tp"), None), P("fs", "tp"), P("fs", "tp"), P("fs")),
        out_specs=(P(("grp", "tp"), "fs"), P("grp", "fs"), P(("grp", "fs"), None)),
        check_vma=False,
    )
```

profile of v0, /device:TPU:0, one launch (start us, length us, event | category | flops | bytes accessed | tf_op | source)
XLA Modules:
  0.0 525.0 jit_solution(6429137152449388254)
XLA Ops:
  7.2 0.0 all-gather.3.cloned.1.call-start
  7.2 5.1 multiply_convert_fusion
  12.3 57.8 %all_to_all.29 = bf16[4,192,3072]{2,1,0:T(8,128)(2,1)S(1)} all-to-all(bf16[4,192,3072]{2,1,0:T(8,128)(2,1)S(1)} %bitcast.13), channel_id=1, replica_groups=mesh['grp'=2,'fs'=4,'tp'=4] {'tp'}, dimensions={0} | all-to-all | bytes 9437184 | tf_op jit(solution)/shard_map/all_to_all | solution.py:17
  70.1 108.8 %all_to_all.30 = bf16[192,4,3072]{2,0,1:T(8,128)(2,1)} all-to-all(bf16[192,4,3072]{2,0,1:T(8,128)(2,1)S(1)} %bitcast.12), channel_id=1, replica_groups=mesh['grp'=2,'fs'=4,'tp'=4] {'fs'}, dimensions={1} | all-to-all | bytes 9437184 | tf_op jit(solution)/shard_map/all_to_all | solution.py:18
  178.9 0.0 all-gather.3.cloned.1.call-update
  178.9 0.0 all-gather.5.cloned.1.call-start
  179.0 6.7 %convert_element_type.22 = bf16[3072,768]{1,0:T(8,128)(2,1)} convert(f32[3072,768]{1,0:T(8,128)} %param.6) | non-fusion elementwise | flops 2359296 | bytes 14155776 | tf_op jit(solution)/shard_map/convert_element_type | solution.py:16
  185.7 0.0 copy-start
  185.7 0.0 all-gather.5.cloned.1.call-update
  185.7 0.0 reduce-scatter.2.cloned.1.call-start
  185.8 1.7 copy-done
  187.5 0.3 convert_reduce_fusion
  187.8 0.6 fusion.4
  188.4 108.7 %all-gather.3.cloned.1.call-done = bf16[4,768,3072]{2,1,0:T(8,128)(2,1)} async-done(((bf16[4,192,3072]{2,1,0:T(8,128)(2,1)}), bf16[4,768,3072]{2,1,0:T(8,128)(2,1)}) %all-gather.3.cloned.1.call-update) | async-done | bytes 18874384 | tf_op jit(solution)/shard_map/all_gather | solution.py:22
  297.0 9.4 %fusion.1 = bf16[256,3072]{1,0:T(8,128)(2,1)S(1)} fusion(bf16[3072,3072]{1,0:T(8,128)(2,1)} %bitcast.7, bf16[256,3072]{1,0:T(8,128)(2,1)S(1)} %copy-done, f32[256]{0:T(256)S(1)} %add_rsqrt_fusion, f32[256]{0:T(256)S(1)} %broadcast_multiply_fusion), kind=kOutput, calls=%fused_computation.5 | convolution fusion | flops 4837343232 | bytes 22022144 | tf_op jit(solution)/shard_map/dot_general | solution.py:27
  306.5 112.7 %all-gather.5.cloned.1.call-done = bf16[3072,3072]{1,0:T(8,128)(2,1)} async-done(((bf16[3072,768]{1,0:T(8,128)(2,1)}), bf16[3072,3072]{1,0:T(8,128)(2,1)}) %all-gather.5.cloned.1.call-update) | async-done | bytes 18874384 | tf_op jit(solution)/shard_map/all_gather | solution.py:23
  419.2 10.7 %fusion.9 = f32[256,3072]{1,0:T(8,128)} fusion(bf16[256,3072]{1,0:T(8,128)(2,1)S(1)} %fusion.1, bf16[3072,3072]{1,0:T(8,128)(2,1)} %all-gather.5.cloned.1.call-done), kind=kOutput, calls=%fused_computation.14 | convolution fusion | flops 4831838208 | bytes 23592960 | tf_op jit(solution)/shard_map/dot_general | solution.py:29
  429.9 0.0 reduce-scatter.2.cloned.1.call-update
  429.9 60.6 %reduce-scatter.2.cloned.1.call-done = f32[256,768]{1,0:T(8,128)} async-done(((f32[256,3072]{1,0:T(8,128)}), f32[256,768]{1,0:T(8,128)}) %reduce-scatter.2.cloned.1.call-update) | async-done | bytes 786448 | tf_op jit(solution)/shard_map/reduce_scatter | solution.py:30
  490.4 0.0 slice-start
  490.4 2.1 convert_element_type.23
  492.5 0.0 slice-start.1
  492.5 0.0 slice-start.2
  492.5 0.0 slice-start.3
  492.5 0.0 slice-start.4
  492.5 19.1 %copy.9 = bf16[3072,3072]{1,0:T(8,128)(2,1)} copy(bf16[3072,3072]{1,0:T(8,128)(2,1)} %bitcast.8) | data formatting | bytes 37748736
  511.6 0.0 slice-done
  511.6 0.0 slice-done.1
  511.6 0.0 slice-done.2
  511.6 0.0 slice-done.3
  511.6 0.0 slice-done.4
  511.6 6.9 %copy.10 = bf16[3072,3072]{1,0:T(8,128)(2,1)} copy(bf16[3072,3072]{1,0:T(8,128)(2,1)S(1)} %bitcast.10) | data formatting | bytes 37748736
  (3 shorter events, 0.0 us)
Async XLA Ops:
  7.2 289.9 %all-gather.3.cloned.1.call-start = ((), (), s32[]{:S(2)}) async-start(), calls=%async_computation.3 | async-start | bytes 23592960 | tf_op jit(solution)/shard_map/all_gather | solution.py:22
  178.9 240.2 %all-gather.5.cloned.1.call-start = ((), (), s32[]{:S(2)}) async-start(), calls=%async_computation.4 | async-start | bytes 23592960 | tf_op jit(solution)/shard_map/all_gather | solution.py:23
  185.7 1.8 copy-start
  185.7 304.7 %reduce-scatter.2.cloned.1.call-start = ((), (), s32[]{:S(2)}) async-start(), calls=%async_computation.5 | async-start | bytes 3932160 | tf_op jit(solution)/shard_map/reduce_scatter | solution.py:30
  490.4 21.2 %slice-start = ((s8[18874368]{0:T(1024)(128)(4,1)}), s8[4194304]{0:T(1024)(128)(4,1)S(1)}, s32[]{:S(2)}) async-start(s8[18874368]{0:T(1024)(128)(4,1)} %bitcast.9), calls=%async_computation.6 | async-start | bytes 8388608
  492.5 19.1 %slice-start.1 = ((s8[18874368]{0:T(1024)(128)(4,1)}), s8[4194304]{0:T(1024)(128)(4,1)S(1)}, s32[]{:S(2)}) async-start(s8[18874368]{0:T(1024)(128)(4,1)} %bitcast.9), calls=%async_computation.7 | async-start | bytes 8388608
  492.5 19.1 %slice-start.2 = ((s8[18874368]{0:T(1024)(128)(4,1)}), s8[4194304]{0:T(1024)(128)(4,1)S(1)}, s32[]{:S(2)}) async-start(s8[18874368]{0:T(1024)(128)(4,1)} %bitcast.9), calls=%async_computation.8 | async-start | bytes 8388608
  492.5 19.1 %slice-start.3 = ((s8[18874368]{0:T(1024)(128)(4,1)}), s8[4194304]{0:T(1024)(128)(4,1)S(1)}, s32[]{:S(2)}) async-start(s8[18874368]{0:T(1024)(128)(4,1)} %bitcast.9), calls=%async_computation.9 | async-start | bytes 8388608
  492.5 19.1 %slice-start.4 = ((s8[18874368]{0:T(1024)(128)(4,1)}), s8[2097152]{0:T(1024)(128)(4,1)S(1)}, s32[]{:S(2)}) async-start(s8[18874368]{0:T(1024)(128)(4,1)} %bitcast.9), calls=%async_computation.10 | async-start | bytes 4194304
Sparse Core Ops, SparseCore 0:
  179.1 117.9 all-gather.2
  299.2 119.9 all-gather.4
  430.0 60.3 reduce-scatter.1
where the time goes:
time: 525 us
  waiting for transfers between devices  282 us (54%)
  blocking collectives  167 us (32%)
  local copies, waits for them, and re-layouts  27.7 us (5%)
  matrix products  20.1 us (4%)
  other arithmetic  14.7 us (3%)
  between operations  13.8 us (3%)
    all_gather x1, waiting for transfers between devices, shards(): lax.all_gather(down_cast, 'tp', axis=1, tiled=True)  113 us
    all_to_all x1, blocking collectives, shards(): lax.all_to_all(quarter, 'fs', split_axis=1, concat_axis=0, tiled=True)  109 us
    all_gather x1, waiting for transfers between devices, shards(): lax.all_gather(stacked, 'tp', axis=1, tiled=True)  109 us
    reduce_scatter x1, waiting for transfers between devices, shards(): summed = lax.psum_scatter(terms, 'fs', scatter_dimension=1, tiled=True)  60.6 us
    all_to_all x1, blocking collectives, shards(): lax.all_to_all(up_cast, 'tp', split_axis=0, concat_axis=1, tiled=True)  57.8 us
    unnamed x14, local copies, waits for them, and re-layouts  27.7 us
    dot_general x1, matrix products, shards(): terms = jnp.dot(hidden, sampled_down, preferred_element_type=jnp.float32)  10.7 us
  transfers between devices with their start and end apart: 3, of which 3 were waited for; matrix products, arithmetic and copies ran while one was open for 3% of the time, Pallas kernels for 0%

commit v1 on v0

--- a/solution.py
+++ b/solution.py
@@ -19,7 +19,7 @@
     part_rows = quarter.shape[0]
     stacked = moved.reshape(moved.shape[0] // part_rows, part_rows, moved.shape[1])
     joined, sampled_down = (
-        lax.all_gather(stacked, "tp", axis=1, tiled=True),
+        jnp.concatenate(lax.all_gather(stacked, "tp"), axis=1),
         lax.all_gather(down_cast, "tp", axis=1, tiled=True),
     )
     sampled_up = joined.reshape(joined.shape[0] * joined.shape[1], joined.shape[2])

time: 525 us -> 517 us (0.985)
  waiting for transfers between devices: 282 us -> 266 us
  local copies, waits for them, and re-layouts: 27.7 us -> 38.9 us
    all_gather x1, waiting for transfers between devices: 113 us -> 96.1 us  [shards(): lax.all_gather(down_cast, 'tp', axis=1, tiled=True)]
    reshape x0 -> x1, local copies, waits for them, and re-layouts: none -> 10.1 us  [shards(): jnp.concatenate(lax.all_gather(stacked, 'tp'), axis=1)]
    unnamed x14 -> x5, local copies, waits for them, and re-layouts: 27.7 us -> 28.9 us
  transfers between devices with their start and end apart: 3 -> 3, of which waited for: 3 -> 3; matrix products, arithmetic and copies ran while one was open for 3% -> 4% of each run, Pallas kernels for 0% -> 0%
where the time goes in v1:
time: 517 us; the launch traced here: 516 us
  waiting for transfers between devices  266 us (51%)
  blocking collectives  167 us (32%)
  local copies, waits for them, and re-layouts  38.9 us (8%)
  matrix products  16 us (3%)
  other arithmetic  14.5 us (3%)
  between operations  13.8 us (3%)
    all_gather x1, waiting for transfers between devices, shards(): lax.all_gather(stacked, 'tp')  110 us
    all_to_all x1, blocking collectives, shards(): lax.all_to_all(quarter, 'fs', split_axis=1, concat_axis=0, tiled=True)  109 us
    all_gather x1, waiting for transfers between devices, shards(): lax.all_gather(down_cast, 'tp', axis=1, tiled=True)  96.1 us
    reduce_scatter x1, waiting for transfers between devices, shards(): summed = lax.psum_scatter(terms, 'fs', scatter_dimension=1, tiled=True)  60.6 us
    all_to_all x1, blocking collectives, shards(): lax.all_to_all(up_cast, 'tp', split_axis=0, concat_axis=1, tiled=True)  57.8 us
    unnamed x5, local copies, waits for them, and re-layouts  28.9 us
    dot_general x1, matrix products, shards(): terms = jnp.dot(hidden, sampled_down, preferred_element_type=jnp.float32)  10.7 us
  transfers between devices with their start and end apart: 3, of which 3 were waited for; matrix products, arithmetic and copies ran while one was open for 4% of the time, Pallas kernels for 0%

profile of v1, /device:TPU:0, one launch (start us, length us, event | category | flops | bytes accessed | tf_op | source)
XLA Modules:
  0.0 516.2 jit_solution(2515850050477024355)
XLA Ops:
  7.2 0.0 all-gather.6.cloned.1.call-start
  7.2 5.1 multiply_convert_fusion
  12.3 57.8 %all_to_all.29 = bf16[4,192,3072]{2,1,0:T(8,128)(2,1)S(1)} all-to-all(bf16[4,192,3072]{2,1,0:T(8,128)(2,1)S(1)} %bitcast.15), channel_id=1, replica_groups=mesh['grp'=2,'fs'=4,'tp'=4] {'tp'}, dimensions={0} | all-to-all | bytes 9437184 | tf_op jit(solution)/shard_map/all_to_all | solution.py:17
  70.1 108.8 %all_to_all.30 = bf16[192,4,3072]{2,0,1:T(8,128)(2,1)} all-to-all(bf16[192,4,3072]{2,0,1:T(8,128)(2,1)S(1)} %bitcast.14), channel_id=1, replica_groups=mesh['grp'=2,'fs'=4,'tp'=4] {'fs'}, dimensions={1} | all-to-all | bytes 9437184 | tf_op jit(solution)/shard_map/all_to_all | solution.py:18
  178.9 0.0 all-gather.6.cloned.1.call-update
  178.9 0.0 all-gather.4.cloned.1.call-start
  179.0 6.6 %convert_element_type.22 = bf16[3072,768]{1,0:T(8,128)(2,1)} convert(f32[3072,768]{1,0:T(8,128)} %param.6) | non-fusion elementwise | flops 2359296 | bytes 14155776 | tf_op jit(solution)/shard_map/convert_element_type | solution.py:16
  185.6 0.0 copy-start.1
  185.6 0.0 all-gather.4.cloned.1.call-update
  185.6 0.0 reduce-scatter.2.cloned.1.call-start
  185.7 1.7 copy-done.1
  187.3 0.3 convert_reduce_fusion
  187.6 0.6 fusion.4
  188.2 109.6 %all-gather.6.cloned.1.call-done = bf16[16,192,3072]{2,1,0:T(8,128)(2,1)} async-done(((bf16[4,192,3072]{2,1,0:T(8,128)(2,1)}), bf16[16,192,3072]{2,1,0:T(8,128)(2,1)}) %all-gather.6.cloned.1.call-update) | async-done | bytes 18874384 | tf_op jit(solution)/shard_map/all_gather | solution.py:22
  297.8 10.1 %copy.8 = bf16[4,4,192,3072]{3,2,1,0:T(8,128)(2,1)S(1)} copy(bf16[4,4,192,3072]{3,2,0,1:T(8,128)(2,1)} %bitcast.12) | data formatting | bytes 37748736 | tf_op jit(solution)/shard_map/reshape | solution.py:22
  307.9 0.0 copy-start
  307.9 10.6 %copy-done = bf16[4,4,192,3072]{3,2,1,0:T(8,128)(2,1)} copy-done((bf16[4,4,192,3072]{3,2,1,0:T(8,128)(2,1)}, bf16[4,4,192,3072]{3,2,1,0:T(8,128)(2,1)S(1)}, u32[]{:S(2)}) %copy-start) | copy-done | bytes 18874392
  318.5 5.3 %fusion.1 = bf16[256,3072]{1,0:T(8,128)(2,1)S(1)} fusion(bf16[3072,3072]{1,0:T(8,128)(2,1)S(1)} %bitcast.10, bf16[256,3072]{1,0:T(8,128)(2,1)S(1)} %copy-done.1, f32[256]{0:T(256)S(1)} %add_rsqrt_fusion, f32[256]{0:T(256)S(1)} %broadcast_multiply_fusion), kind=kOutput, calls=%fused_computation.5 | convolution fusion | flops 4837343232 | bytes 22022144 | tf_op jit(solution)/shard_map/dot_general | solution.py:27
  323.8 96.1 %all-gather.4.cloned.1.call-done = bf16[3072,3072]{1,0:T(8,128)(2,1)} async-done(((bf16[3072,768]{1,0:T(8,128)(2,1)}), bf16[3072,3072]{1,0:T(8,128)(2,1)}) %all-gather.4.cloned.1.call-update) | async-done | bytes 18874384 | tf_op jit(solution)/shard_map/all_gather | solution.py:23
  420.0 10.7 %fusion.9 = f32[256,3072]{1,0:T(8,128)} fusion(bf16[256,3072]{1,0:T(8,128)(2,1)S(1)} %fusion.1, bf16[3072,3072]{1,0:T(8,128)(2,1)} %all-gather.4.cloned.1.call-done), kind=kOutput, calls=%fused_computation.14 | convolution fusion | flops 4831838208 | bytes 23592960 | tf_op jit(solution)/shard_map/dot_general | solution.py:29
  430.6 0.0 reduce-scatter.2.cloned.1.call-update
  430.6 60.6 %reduce-scatter.2.cloned.1.call-done = f32[256,768]{1,0:T(8,128)} async-done(((f32[256,3072]{1,0:T(8,128)}), f32[256,768]{1,0:T(8,128)}) %reduce-scatter.2.cloned.1.call-update) | async-done | bytes 786448 | tf_op jit(solution)/shard_map/reduce_scatter | solution.py:30
  491.2 1.9 convert_element_type.23
  493.1 16.6 %copy.10 = bf16[3072,3072]{1,0:T(8,128)(2,1)} copy(bf16[3072,3072]{1,0:T(8,128)(2,1)} %all-gather.4.cloned.1.call-done) | data formatting | bytes 37748736
  (2 shorter events, 0.0 us)
Async XLA Ops:
  7.2 290.6 %all-gather.6.cloned.1.call-start = ((), (), s32[]{:S(2)}) async-start(), calls=%async_computation.5 | async-start | bytes 23592960 | tf_op jit(solution)/shard_map/all_gather | solution.py:22
  178.9 241.0 %all-gather.4.cloned.1.call-start = ((), (), s32[]{:S(2)}) async-start(), calls=%async_computation.3 | async-start | bytes 23592960 | tf_op jit(solution)/shard_map/all_gather | solution.py:23
  185.6 1.7 copy-start.1
  185.6 305.6 %reduce-scatter.2.cloned.1.call-start = ((), (), s32[]{:S(2)}) async-start(), calls=%async_computation.4 | async-start | bytes 3932160 | tf_op jit(solution)/shard_map/reduce_scatter | solution.py:30
  307.9 10.6 %copy-start = (bf16[4,4,192,3072]{3,2,1,0:T(8,128)(2,1)}, bf16[4,4,192,3072]{3,2,1,0:T(8,128)(2,1)S(1)}, u32[]{:S(2)}) copy-start(bf16[4,4,192,3072]{3,2,1,0:T(8,128)(2,1)S(1)} %copy.8) | copy-start | bytes 56623108
Sparse Core Ops, SparseCore 0:
  179.1 118.6 all-gather.5
  299.9 119.9 all-gather.3
  430.8 60.3 reduce-scatter.1
